TPU v7x, 32 devices: a whole 2x2x4 slice. The times are simulated.
32 devices in a mesh: ep: 8 (over z, core), tp: 4 (over y, x).
Axes of the slice: x: 2, y: 2, z: 4, core: 2. Of those that a mesh axis runs over, the one named last changes fastest.
Arguments:
- outer_gate: bfloat16 [1024, 2048], P('ep', 'tp'), may hold values from -6 to 6
- inner_gate: bfloat16 [1024, 2048], P('ep', 'tp'), may hold values from -6 to 6
- conv_value: bfloat16 [1024, 2048], P('ep', 'tp'), may hold values from -6 to 6
- conv_taps: bfloat16 [3, 2048], P(None, 'tp'), may hold values from -3.5 to 3.5
- mix_out: bfloat16 [2048, 2048], P(None, 'tp')
- gain_mixer: bfloat16 [2048], P('tp'), may hold values from 0.099609375 to 1.8984375
- bias_mixer: bfloat16 [2048], P('tp'), may hold values from -3 to 3
- moe_input: bfloat16 [1024, 2048], P('ep'), may hold values from -6 to 6
- route_ids: int32 [1024, 4], P('ep'), may hold values from 0 to 7, all different within a row; in each aligned block of 128 rows (0 to 127, 128 to 255, ...) at most 96 rows name the same one
- route_weights: float32 [1024, 4], P('ep'), may hold values from 0.1 to 1.2
- expert_gate: bfloat16 [8, 2048, 2048], P('ep', None, 'tp'), may hold values from -0.125 to 0.125
- expert_up: bfloat16 [8, 2048, 2048], P('ep', None, 'tp'), may hold values from -0.125 to 0.125
- expert_down: bfloat16 [8, 2048, 2048], P('ep', None, 'tp')
- shared_gate: bfloat16 [2048, 2048], P(None, 'tp'), may hold values from -0.125 to 0.125
- shared_up: bfloat16 [2048, 2048], P(None, 'tp'), may hold values from -0.125 to 0.125
- shared_down: bfloat16 [2048, 2048], P(None, 'tp')
- gain_experts: bfloat16 [2048], P('tp'), may hold values from 0.099609375 to 1.8984375
- bias_experts: bfloat16 [2048], P('tp'), may hold values from -3 to 3
Outputs:
- out_mixer: bfloat16 [1024, 2048], P('ep', 'tp')
- out_experts: bfloat16 [1024, 2048], P('ep', 'tp')
Inputs may be any that keep to these rules, and one draw needn't show every extreme that they name: `route_ids`: each row names 4 different experts. Among the rows of one index of ep (aligned blocks of 128 rows) no expert is named more than 96 times, a bound that some block reaches.
All inputs are finite; a program needn't handle non-finite values.
Results may differ from a plain program's by a relative error of at most 0.0055.
Values may be sent and summed in bfloat16 or wider, within the bound.
A program may use at most 64 MiB of HBM per device.

v0:
```python
import functools

import jax
import jax.numpy as jnp
from jax import lax
from jax.experimental import pallas as pl
from jax.experimental.pallas import tpu as pltpu
from jax.sharding import PartitionSpec as P

SEQS = 1


def shifted(block, axis, distance):
    devices = range(lax.axis_size(axis))
    route = [(i - distance, i) for i in devices if i - distance in devices]
    return lax.ppermute(block, axis, route)


def finish(values, totals, squares, full_width, gain, offset_bias):
    average = (totals / full_width)[:, None]
    spread = (squares / full_width)[:, None] - average * average
    scaled = (values - average) * lax.rsqrt(spread + 1e-05)
    return (scaled * gain.astype(jnp.float32) + offset_bias.astype(jnp.float32)).astype(
        jnp.bfloat16
    )


def plain_device(
    outer_gate,
    inner_gate,
    conv_value,
    conv_taps,
    mix_out,
    gain_mixer,
    bias_mixer,
    moe_input,
    route_ids,
    route_weights,
    expert_gate,
    expert_up,
    expert_down,
    shared_gate,
    shared_up,
    shared_down,
    gain_experts,
    bias_experts,
):
    token_rows = outer_gate.shape[0]
    column_count = outer_gate.shape[1]
    ep_count = lax.axis_size("ep")
    tp_count = lax.axis_size("tp")
    taps_count = conv_taps.shape[0]
    product = (inner_gate.astype(jnp.float32) * conv_value.astype(jnp.float32)).astype(jnp.bfloat16)
    border = shifted(product[token_rows - (taps_count - 1) :], "ep", 1)
    extended = jnp.concatenate([border, product], axis=0).astype(jnp.float32)
    seq_length = token_rows * ep_count // SEQS
    places = (
        lax.axis_index("ep") * token_rows + jnp.arange(token_rows, dtype=jnp.int32)
    ) % seq_length
    convolved = jnp.zeros((token_rows, column_count), jnp.float32)
    for offset in range(taps_count):
        delay_rows = taps_count - 1 - offset
        delayed = extended[offset : offset + token_rows]
        kept_mask = (places >= delay_rows).astype(jnp.float32)[:, None]
        convolved = convolved + conv_taps[offset].astype(jnp.float32)[None, :] * delayed * kept_mask
    weighted_in = (outer_gate.astype(jnp.float32) * convolved).astype(jnp.bfloat16)
    block = mix_out
    mixed = jnp.dot(
        lax.all_gather(weighted_in, "tp", axis=1, tiled=True),
        block,
        preferred_element_type=jnp.float32,
    )
    topk_count = route_ids.shape[1]
    local_experts = expert_gate.shape[0]
    expert_count = local_experts * ep_count
    capacity = max(2, 3 * token_rows * topk_count // (2 * expert_count))
    flat_ids = route_ids.reshape(-1)
    marks = (flat_ids[:, None] == jnp.arange(expert_count, dtype=jnp.int32)[None, :]).astype(
        jnp.int32
    )
    ranks = jnp.sum((jnp.cumsum(marks, axis=0) - marks) * marks, axis=1)
    targets = flat_ids * capacity + ranks
    sources = jnp.arange(flat_ids.shape[0], dtype=jnp.int32) // topk_count
    sent_rows = lax.dynamic_slice_in_dim(
        moe_input, lax.axis_index("tp") * column_count, column_count, 1
    )
    buffer_rows = jnp.zeros((expert_count * capacity, sent_rows.shape[1]), jnp.bfloat16)
    buffer_rows = buffer_rows.at[targets].set(sent_rows[sources])
    sectioned = buffer_rows.reshape(ep_count, local_experts * capacity, sent_rows.shape[1])
    arrived = lax.all_to_all(sectioned, "ep", split_axis=0, concat_axis=0, tiled=True)
    arrived = lax.all_gather(arrived, "tp", axis=2, tiled=True)
    expert_rows = arrived.reshape(ep_count, local_experts, capacity, arrived.shape[2])
    gate_value = jnp.einsum(
        "secd,edf->secf", expert_rows, expert_gate, preferred_element_type=jnp.float32
    )
    up_value = jnp.einsum(
        "secd,edf->secf", expert_rows, expert_up, preferred_element_type=jnp.float32
    )
    hidden = (jax.nn.silu(gate_value) * up_value).astype(jnp.bfloat16)
    flat_hidden = hidden.reshape(expert_count * capacity, hidden.shape[3])
    shared_gate_value = jnp.dot(moe_input, shared_gate, preferred_element_type=jnp.float32)
    shared_up_value = jnp.dot(moe_input, shared_up, preferred_element_type=jnp.float32)
    shared_hidden = (jax.nn.silu(shared_gate_value) * shared_up_value).astype(jnp.bfloat16)
    piece = lax.all_gather(flat_hidden, "tp", axis=1, tiled=True)
    block = expert_down
    shaped = piece.reshape(ep_count, local_experts, capacity, piece.shape[1])
    routed_sum = jnp.einsum("secf,efd->secd", shaped, block, preferred_element_type=jnp.float32)
    block = shared_down
    shared_sum = jnp.dot(
        lax.all_gather(shared_hidden, "tp", axis=1, tiled=True),
        block,
        preferred_element_type=jnp.float32,
    )
    expert_out = routed_sum.astype(jnp.bfloat16).reshape(
        ep_count, local_experts * capacity, column_count
    )
    returned = lax.all_to_all(expert_out, "ep", split_axis=0, concat_axis=0, tiled=True)
    picked = returned.reshape(expert_count * capacity, column_count)[targets].astype(jnp.float32)
    weighted = picked.reshape(token_rows, topk_count, column_count) * route_weights[:, :, None]
    combined = jnp.sum(weighted, axis=1) + shared_sum
    mixer_total, mixer_square, expert_total, expert_square = lax.psum(
        (
            jnp.sum(mixed, axis=1),
            jnp.sum(mixed * mixed, axis=1),
            jnp.sum(combined, axis=1),
            jnp.sum(combined * combined, axis=1),
        ),
        "tp",
    )
    full_width = column_count * tp_count
    out_mixer = finish(mixed, mixer_total, mixer_square, full_width, gain_mixer, bias_mixer)
    out_experts = finish(
        combined, expert_total, expert_square, full_width, gain_experts, bias_experts
    )
    return (out_mixer, out_experts)


PLANE = 2
CORES = 2
VMEM_BYTES = 60 * 1024 * 1024


def plan(chips):
    steps = [("shared", 0), ("up", 0), ("hidden", 0)]
    waiting = [("shared_relay", 0)]
    for s in range(1, chips):
        steps.append(("line", s))
        steps += waiting
        waiting = [("token_relay", 1), ("hidden_relay", 0)] if s == 1 else []
    steps += waiting + [("mixer", 0)]
    for s in range(1, chips):
        steps.append(("pair", s))
        if s + 1 < chips:
            steps.append(("token_relay", s + 1))
        if s == min(2, chips - 1):
            steps.append(("mixer_relay", 0))
        steps += [("up", s), ("hidden", s)]
        if s == chips - 1:
            steps.append(("mixer_dot", 0))
        if s > 1:
            steps.append(("hidden_relay", s - 1))
    steps.append(("shared_dot", 0))
    for s in range(chips):
        steps.append(("down", s))
        if s == 0:
            steps.append(("hidden_relay", chips - 1))
        if s == chips - 2:
            steps.append(("mixer_end", 0))
        steps.append(("return", s))
    return steps + [("collect", s) for s in range(1, chips)]


def silu(value):
    return value / (1.0 + jnp.exp(-value))


def fused_kernel(
    shape,
    outer_ref,
    inner_ref,
    value_ref,
    taps_ref,
    mix_hbm,
    gain_m_ref,
    bias_m_ref,
    moe_ref,
    ids_ref,
    route_w_ref,
    gate_hbm,
    up_hbm,
    down_hbm,
    shared_gate_hbm,
    shared_up_hbm,
    shared_down_hbm,
    gain_e_ref,
    bias_e_ref,
    out_m_ref,
    out_e_ref,
    mix_v,
    gate_v,
    up_v,
    down_v,
    shared_gate_v,
    shared_up_v,
    shared_down_v,
    tokens,
    route,
    rows_in,
    hidden,
    weighted,
    shared_hidden,
    border,
    edge,
    extended,
    peer_part,
    own_part,
    sent_sum,
    returned,
    stats_out,
    stats_in,
    mixed_ref,
    total_ref,
    load_sem,
    send_sem,
    recv_sem,
):
    ep_count, tp_count, capacity, seq_length = shape
    chips = ep_count // CORES
    rows, cols = outer_ref.shape
    full_width = cols * tp_count
    me = lax.axis_index("ep")
    j = lax.axis_index("tp")
    z = me // CORES
    c = me % CORES
    x = j % PLANE
    y = j // PLANE
    jx = y * PLANE + (1 - x)
    jy = (1 - y) * PLANE + x
    jd = (1 - y) * PLANE + (1 - x)
    other = z * CORES + (1 - c)
    f32, bf16 = jnp.float32, jnp.bfloat16

    order = (
        (shared_gate_hbm, shared_gate_v),
        (shared_up_hbm, shared_up_v),
        (gate_hbm.at[0], gate_v),
        (up_hbm.at[0], up_v),
        (mix_hbm, mix_v),
        (down_hbm.at[0], down_v),
        (shared_down_hbm, shared_down_v),
    )
    loads = [pltpu.make_async_copy(a, b, load_sem.at[n]) for n, (a, b) in enumerate(order)]
    for load in loads:
        load.start()

    product = (inner_ref[...].astype(f32) * value_ref[...].astype(f32)).astype(bf16)
    edge_rows = edge.shape[0]
    edge[...] = product[rows - edge_rows :]
    pad = extended.shape[0] - rows
    extended[pad:, :] = product.astype(f32)
    named = lax.broadcasted_iota(jnp.int32, (ep_count, rows), 0)
    dense = jnp.zeros((ep_count, rows), f32)
    for k in range(ids_ref.shape[0]):
        dense = dense + jnp.where(named == ids_ref[k : k + 1, :], route_w_ref[k : k + 1, :], 0.0)
    route[0, 0] = dense

    barrier = pltpu.get_barrier_semaphore()
    for step in range(1, ep_count):
        pl.semaphore_signal(barrier, inc=1, device_id=((me + step) % ep_count, j), device_id_type=pl.DeviceIdType.MESH)
    for peer in (jx, jy, jd):
        pl.semaphore_signal(barrier, inc=1, device_id=(me, peer), device_id_type=pl.DeviceIdType.MESH)
    pl.semaphore_wait(barrier, ep_count - 1 + tp_count - 1)

    numbers = {}
    started = []

    def number(name):
        return numbers.setdefault(name, len(numbers))

    def copy(name, source, target, device):
        n = number(name)
        return pltpu.make_async_remote_copy(
            src_ref=source,
            dst_ref=target,
            send_sem=send_sem.at[n],
            recv_sem=recv_sem.at[n],
            device_id=device,
            device_id_type=pl.DeviceIdType.MESH,
        )

    def send(name, source, target, device):
        c_ = copy(name, source, target, device)
        c_.start()
        started.append(c_)

    def arrive(name, target):
        copy(name, target, target, (other, j)).wait_recv()

    def columns(owner):
        return pl.ds(pl.multiple_of(owner * cols, cols), cols)

    def gather_start(name, ref):
        part = ref.at[:, columns(j)]
        send(name + ("x",), part, part, (me, jx))
        send(name + ("y",), part, part, (me, jy))

    def gather_relay(name, ref):
        half = ref.shape[0] // 2
        arrive(name + ("x",), ref.at[:, columns(jx)])
        part = ref.at[pl.ds(0, half), columns(jx)]
        send(name + ("xy",), part, part, (me, jy))
        arrive(name + ("y",), ref.at[:, columns(jy)])
        part = ref.at[pl.ds(half, half), columns(jy)]
        send(name + ("yx",), part, part, (me, jx))

    def gather_finish(name, ref):
        half = ref.shape[0] // 2
        arrive(name + ("xy",), ref.at[pl.ds(0, half), columns(jd)])
        arrive(name + ("yx",), ref.at[pl.ds(half, half), columns(jd)])

    send(("pair", 0), moe_ref, tokens.at[0, 1], (other, j))
    for s in range(chips):
        target = (z - s + chips) % chips
        if s > 0:
            send(("route", s, 0), route.at[0, 0], route.at[s, 0], (target * CORES + c, j))
        send(("route", s, 1), route.at[0, 0], route.at[s, 1], (target * CORES + (1 - c), j))
    for s in range(1, chips):
        target = (z - s + chips) % chips
        send(
            ("line", s),
            moe_ref.at[:, columns(j)],
            tokens.at[s, 0, :, columns(j)],
            (target * CORES + c, j),
        )
    send(("edge",), edge, border, ((me + 1) % ep_count, j))

    def dot(a, b):
        return jnp.dot(a, b, preferred_element_type=f32)

    def token_ref(s, p):
        return moe_ref if (s, p) == (0, 0) else tokens.at[s, p]

    def choice(s, p):
        weight = route[s, p, pl.ds(me, 1), :]
        routed = (weight > 0.0).astype(f32)
        earlier = lax.broadcasted_iota(jnp.int32, (rows, rows), 0)
        later = lax.broadcasted_iota(jnp.int32, (rows, rows), 1)
        upper = (earlier <= later).astype(f32).astype(bf16)
        many = jnp.broadcast_to(routed, (16, rows)).astype(bf16)
        rank = dot(many, upper)[0:1, :] * routed
        slot = lax.broadcasted_iota(jnp.int32, (capacity, rows), 0).astype(f32) + 1.0
        return (slot == rank).astype(f32), weight

    def expert_up_stage(s):
        for p in range(CORES):
            picks, _ = choice(s, p)
            rows_in[p * capacity : (p + 1) * capacity, :] = dot(
                picks.astype(bf16), token_ref(s, p)[...]
            ).astype(bf16)
        held = silu(dot(rows_in[...], gate_v[...])) * dot(rows_in[...], up_v[...])
        hidden[s, :, columns(j)] = held.astype(bf16)

    def hidden_start(s):
        gather_start(("hidden", s), hidden.at[s])

    def hidden_relay(s):
        gather_relay(("hidden", s), hidden.at[s])

    def token_relay(s):
        gather_relay(("tokens", s), tokens.at[s, 0])

    def collect(s):
        arrive(("return", s), returned.at[s])
        total_ref[...] = total_ref[...] + returned[s].astype(f32)

    def expert_down_stage(s):
        full = dot(hidden[s], down_v[...])
        for p in reversed(range(CORES)):
            picks, weight = choice(s, p)
            scale = jnp.sum(picks * weight, axis=1, keepdims=True)
            scaled = (full[p * capacity : (p + 1) * capacity] * scale).astype(bf16)
            spread = lax.dot_general(
                picks.astype(bf16), scaled, (((0,), (0,)), ((), ())), preferred_element_type=f32
            )
            if p == 1:
                own_part[s] = spread.astype(bf16)
                send(("part", s), own_part.at[s], peer_part.at[s], (other, j))
            elif s == 0:
                total_ref[...] = total_ref[...] + spread
            else:
                sent_sum[s] = spread.astype(bf16)

    def expert_return(s):
        arrive(("part", s), peer_part.at[s])
        if s == 0:
            total_ref[...] = total_ref[...] + peer_part[0].astype(f32)
        else:
            sent_sum[s] = (sent_sum[s].astype(f32) + peer_part[s].astype(f32)).astype(bf16)
            target = (z + s) % chips
            send(("return", s), sent_sum.at[s], returned.at[s], (target * CORES + c, j))

    def wait_routes(s):
        for p in range(CORES):
            if (s, p) != (0, 0):
                arrive(("route", s, p), route.at[s, p])

    def pair_tokens(s):
        gather_finish(("tokens", s), tokens.at[s, 0])
        send(("pair", s), tokens.at[s, 0], tokens.at[s, 1], (other, j))

    def line_tokens(s):
        arrive(("line", s), tokens.at[s, 0, :, columns(j)])
        gather_start(("tokens", s), tokens.at[s, 0])

    def stats_start(k, values):
        lane = lax.broadcasted_iota(jnp.int32, (rows, rows), 1)
        total = jnp.sum(values, axis=1, keepdims=True)
        square = jnp.sum(values * values, axis=1, keepdims=True)
        tile = jnp.where(lane == 0, total, jnp.where(lane == 1, square, 0.0))
        stats_out[k] = tile.T[0 : stats_out.shape[1], :]
        for n, peer in enumerate((jx, jy, jd)):
            send(("stats", k, n), stats_out.at[k], stats_in.at[k, n], (me, peer))

    def stats_finish(k, values, gain_ref, bias_ref, out_ref):
        tile = stats_out[k]
        for n in range(tp_count - 1):
            arrive(("stats", k, n), stats_in.at[k, n])
            tile = tile + stats_in[k, n]
        padded = jnp.concatenate(
            [tile, jnp.zeros((rows - tile.shape[0], rows), f32)], axis=0
        ).T
        average = padded[:, 0:1] / full_width
        spread = padded[:, 1:2] / full_width - average * average
        scaled = (values - average) * lax.rsqrt(spread + 1e-05)
        out_ref[...] = (
            scaled * gain_ref[...].astype(f32).reshape(1, cols)
            + bias_ref[...].astype(f32).reshape(1, cols)
        ).astype(bf16)

    def shared_start(_):
        loads[0].wait()
        loads[1].wait()
        held = silu(dot(moe_ref[...], shared_gate_v[...])) * dot(moe_ref[...], shared_up_v[...])
        shared_hidden[:, columns(j)] = held.astype(bf16)
        gather_start(("shared",), shared_hidden)

    def mixer_start(_):
        arrive(("edge",), border)
        extended[pad - edge_rows : pad, :] = border[...].astype(f32)
        places = (me * rows + lax.broadcasted_iota(jnp.int32, (rows, 1), 0)) % seq_length
        taps_count = taps_ref.shape[0]
        convolved = jnp.zeros((rows, cols), f32)
        for offset in range(taps_count):
            delay = taps_count - 1 - offset
            delayed = extended[pad - delay : pad - delay + rows, :]
            kept = (places >= delay).astype(f32)
            convolved = convolved + taps_ref[offset : offset + 1, :].astype(f32) * delayed * kept
        weighted[:, columns(j)] = (outer_ref[...].astype(f32) * convolved).astype(bf16)
        gather_start(("mixer",), weighted)

    def expert_up_start(s):
        wait_routes(s)
        arrive(("pair", s), tokens.at[s, 1])
        if s == 0:
            loads[2].wait()
            loads[3].wait()
        expert_up_stage(s)

    def shared_relay(_):
        gather_relay(("shared",), shared_hidden)

    def mixer_relay(_):
        gather_relay(("mixer",), weighted)

    def mixer_dot(_):
        gather_finish(("mixer",), weighted)
        loads[4].wait()
        mixed_ref[...] = dot(weighted[...], mix_v[...])
        stats_start(0, mixed_ref[...])

    def mixer_end(_):
        stats_finish(0, mixed_ref[...], gain_m_ref, bias_m_ref, out_m_ref)

    def shared_dot(_):
        gather_finish(("shared",), shared_hidden)
        loads[6].wait()
        total_ref[...] = dot(shared_hidden[...], shared_down_v[...])
        loads[5].wait()

    def expert_down(s):
        gather_finish(("hidden", s), hidden.at[s])
        expert_down_stage(s)

    acts = {
        "shared": shared_start,
        "mixer": mixer_start,
        "shared_relay": shared_relay,
        "mixer_relay": mixer_relay,
        "mixer_dot": mixer_dot,
        "mixer_end": mixer_end,
        "shared_dot": shared_dot,
        "line": line_tokens,
        "token_relay": token_relay,
        "pair": pair_tokens,
        "up": expert_up_start,
        "hidden": hidden_start,
        "hidden_relay": hidden_relay,
        "down": expert_down,
        "return": expert_return,
        "collect": collect,
    }
    for act, s in plan(chips):
        acts[act](s)
    stats_start(1, total_ref[...])
    stats_finish(1, total_ref[...], gain_e_ref, bias_e_ref, out_e_ref)
    for item in started:
        item.wait_send()


def pass_kernel(first_ref, second_ref, out_first_ref, out_second_ref):
    out_first_ref[...] = first_ref[...]
    out_second_ref[...] = second_ref[...]


def fused_device(
    outer_gate,
    inner_gate,
    conv_value,
    conv_taps,
    mix_out,
    gain_mixer,
    bias_mixer,
    moe_input,
    route_ids,
    route_weights,
    expert_gate,
    expert_up,
    expert_down,
    shared_gate,
    shared_up,
    shared_down,
    gain_experts,
    bias_experts,
):
    rows, cols = outer_gate.shape
    width = moe_input.shape[1]
    ep_count = lax.axis_size("ep")
    tp_count = lax.axis_size("tp")
    chips = ep_count // CORES
    capacity = max(2, 3 * rows * route_ids.shape[1] // (2 * ep_count))
    seq_length = rows * ep_count // SEQS
    bf16, f32 = jnp.bfloat16, jnp.float32
    vmem = pl.BlockSpec(memory_space=pltpu.VMEM)
    hbm = pl.BlockSpec(memory_space=pl.ANY)
    copies = 16 * chips + 24
    weight = pltpu.VMEM((width, cols), bf16)
    scratch = [
        *([weight] * 7),
        pltpu.VMEM((chips, CORES, rows, width), bf16),
        pltpu.VMEM((chips, CORES, ep_count, rows), f32),
        pltpu.VMEM((CORES * capacity, width), bf16),
        pltpu.VMEM((chips, CORES * capacity, width), bf16),
        pltpu.VMEM((rows, width), bf16),
        pltpu.VMEM((rows, width), bf16),
        pltpu.VMEM((16, cols), bf16),
        pltpu.VMEM((16, cols), bf16),
        pltpu.VMEM((rows + 16, cols), f32),
        pltpu.VMEM((chips, rows, cols), bf16),
        pltpu.VMEM((chips, rows, cols), bf16),
        pltpu.VMEM((chips, rows, cols), bf16),
        pltpu.VMEM((chips, rows, cols), bf16),
        pltpu.VMEM((2, 8, rows), f32),
        pltpu.VMEM((2, tp_count - 1, 8, rows), f32),
        pltpu.VMEM((rows, cols), f32),
        pltpu.VMEM((rows, cols), f32),
        pltpu.SemaphoreType.DMA((7,)),
        pltpu.SemaphoreType.DMA((copies,)),
        pltpu.SemaphoreType.DMA((copies,)),
    ]
    out = jax.ShapeDtypeStruct((rows, cols), bf16)
    first, second = pl.pallas_call(
        functools.partial(fused_kernel, (ep_count, tp_count, capacity, seq_length)),
        out_shape=(out, out),
        in_specs=[vmem] * 4 + [hbm] + [vmem] * 5
        + [hbm] * 6
        + [vmem, vmem],
        out_specs=(vmem, vmem),
        scratch_shapes=scratch,
        compiler_params=pltpu.CompilerParams(
            collective_id=0, has_side_effects=True, vmem_limit_bytes=VMEM_BYTES
        ),
    )(
        outer_gate,
        inner_gate,
        conv_value,
        conv_taps,
        mix_out,
        gain_mixer,
        bias_mixer,
        moe_input,
        route_ids.T,
        route_weights.T,
        expert_gate,
        expert_up,
        expert_down,
        shared_gate,
        shared_up,
        shared_down,
        gain_experts,
        bias_experts,
    )
    return pl.pallas_call(
        pass_kernel, out_shape=(out, out), in_specs=[vmem, vmem], out_specs=(vmem, vmem)
    )(first, second)


def on_device(*arrays):
    local_experts = arrays[10].shape[0]
    square = lax.axis_size("tp") == PLANE * PLANE
    if square and local_experts == 1 and lax.axis_size("ep") % CORES == 0:
        return fused_device(*arrays)
    return plain_device(*arrays)


def solution(mesh):
    in_specs = (
        P("ep", "tp"),
        P("ep", "tp"),
        P("ep", "tp"),
        P(None, "tp"),
        P(None, "tp"),
        P("tp"),
        P("tp"),
        P("ep", None),
        P("ep", None),
        P("ep", None),
        P("ep", None, "tp"),
        P("ep", None, "tp"),
        P("ep", None, "tp"),
        P(None, "tp"),
        P(None, "tp"),
        P(None, "tp"),
        P("tp"),
        P("tp"),
    )
    out_specs = (P("ep", "tp"), P("ep", "tp"))
    return jax.shard_map(
        on_device, mesh=mesh, in_specs=in_specs, out_specs=out_specs, check_vma=False
    )
```

profile of v0, /device:TPU:0, one launch (start us, length us, event | category | flops | bytes accessed | tf_op | source)
XLA Modules:
  0.0 74.1 jit_solution(15353197621077122468)
XLA Ops:
  0.6 71.8 %shard_map.185 = (bf16[128,512]{1,0:T(8,128)(2,1)}, bf16[128,512]{1,0:T(8,128)(2,1)}) custom-call(bf16[128,512]{1,0:T(8,128)(2,1)} %outer_ref.1, bf16[128,512]{1,0:T(8,128)(2,1)} %inner_ref.1, bf16[128,512]{1,0:T(8,128)(2,1)} %value_ref.1, bf16[3,512]{1,0:T(4,128)(2,1)} %taps_ref.1, bf16[2048,512]{1,0:T(8,128)(2,1)} %mix_hbm.1, bf16[512]{0:T(512)(128)(2,1)} %gain_m_ref.1, ...), custom_call_target="tpu_custom_call" | custom-call | tf_op jit(solution)/shard_map/pallas_call | solution.py:581
  72.5 1.7 %shard_map.186 = (bf16[128,512]{1,0:T(8,128)(2,1)}, bf16[128,512]{1,0:T(8,128)(2,1)}) custom-call(bf16[128,512]{1,0:T(8,128)(2,1)} %get-tuple-element.4.first_ref, bf16[128,512]{1,0:T(8,128)(2,1)} %get-tuple-element.5.second_ref), custom_call_target="tpu_custom_call" | custom-call | tf_op jit(solution)/shard_map/pallas_call | solution.py:612
where the time goes:
time: 74.6 us; the launch traced here: 74.1 us
  Pallas kernels  73.5 us (99%)
    pallas_call x1, Pallas kernels, fused_device(): pl.pallas_call(functools.partial(fused_kernel, (ep_count, tp_count, capac...  71.8 us
    pallas_call x1, Pallas kernels, fused_device(): pl.pallas_call(pass_kernel, out_shape=(out, out), in_specs=[vmem, vmem],...  1.68 us

commit v1 on v0

--- a/solution.py
+++ b/solution.py
@@ -1,4 +1,5 @@
 import functools
+import types
 
 import jax
 import jax.numpy as jnp
@@ -140,34 +141,92 @@
 VMEM_BYTES = 60 * 1024 * 1024
 
 
-def plan(chips):
-    steps = [("shared", 0), ("up", 0), ("hidden", 0)]
-    waiting = [("shared_relay", 0)]
-    for s in range(1, chips):
-        steps.append(("line", s))
-        steps += waiting
-        waiting = [("token_relay", 1), ("hidden_relay", 0)] if s == 1 else []
-    steps += waiting + [("mixer", 0)]
-    for s in range(1, chips):
-        steps.append(("pair", s))
-        if s + 1 < chips:
-            steps.append(("token_relay", s + 1))
-        if s == min(2, chips - 1):
-            steps.append(("mixer_relay", 0))
-        steps += [("up", s), ("hidden", s)]
-        if s == chips - 1:
-            steps.append(("mixer_dot", 0))
-        if s > 1:
-            steps.append(("hidden_relay", s - 1))
-    steps.append(("shared_dot", 0))
-    for s in range(chips):
-        steps.append(("down", s))
-        if s == 0:
-            steps.append(("hidden_relay", chips - 1))
-        if s == chips - 2:
-            steps.append(("mixer_end", 0))
-        steps.append(("return", s))
-    return steps + [("collect", s) for s in range(1, chips)]
+(
+    UP,
+    DOWN,
+    NEAR,
+    ROUTE,
+    PAIR,
+    EDGE,
+    CROSS,
+    HIDDEN,
+    SHARED,
+    MIXER,
+    PART,
+    RETURN,
+    STATS,
+    ONWARD,
+) = range(14)
+LINE = 4
+WHOLE = (3,)
+ALL, INNER, OUTER = range(3)
+
+
+def plan(act):
+    return [
+        (ALL, act.shared, ()),
+        (ALL, act.up, (0,)),
+        (ALL, act.start_y, (0,)),
+        (ALL, act.line, (1, 0)),
+        (INNER, act.line, (2, 0)),
+        (ALL, act.start_x, (0,)),
+        (ALL, act.line, (1, 1)),
+        (INNER, act.line, (2, 1)),
+        (OUTER, act.line, (2, 0)),
+        (INNER, act.line, (3, 0)),
+        (ALL, act.cross, (1, 2)),
+        (ALL, act.cross, (1, 3)),
+        (OUTER, act.line, (2, 1)),
+        (INNER, act.line, (3, 1)),
+        (INNER, act.cross, (2, 2)),
+        (ALL, act.shared_relay, ()),
+        (ALL, act.up, (1,)),
+        (ALL, act.start, (1,)),
+        (INNER, act.cross, (2, 3)),
+        (OUTER, act.line, (3, 0)),
+        (OUTER, act.cross, (2, 2)),
+        (INNER, act.cross, (3, 2)),
+        (OUTER, act.cross, (2, 3)),
+        (OUTER, act.line, (3, 1)),
+        (ALL, act.up, (2,)),
+        (ALL, act.start, (2,)),
+        (INNER, act.cross, (3, 3)),
+        (ALL, act.relay, (1,)),
+        (ALL, act.shared_dot, ()),
+        (OUTER, act.cross, (3, 2)),
+        (OUTER, act.cross, (3, 3)),
+        (ALL, act.up_part, (3, 0)),
+        (ALL, act.start_part, (3, 0)),
+        (ALL, act.relay, (2,)),
+        (ALL, act.up_part, (3, 1)),
+        (ALL, act.start_part, (3, 1)),
+        (ALL, act.down, (1,)),
+        (ALL, act.give_back, (1,)),
+        (ALL, act.relay_part, (3, 0)),
+        (ALL, act.down, (2,)),
+        (ALL, act.relay_part, (3, 1)),
+        (ALL, act.give_back, (2,)),
+        (ALL, act.mixer, ()),
+        (ALL, act.relay, (0,)),
+        (ALL, act.down_part, (3, 0)),
+        (ALL, act.give_back_part, (3, 0)),
+        (ALL, act.down_part, (3, 1)),
+        (ALL, act.give_back_part, (3, 1)),
+        (ALL, act.mixer_relay, ()),
+        (ALL, act.down, (0,)),
+        (ALL, act.give_back, (0,)),
+        (ALL, act.mixer_dot, ()),
+        (ALL, act.collect, (1,)),
+        (ALL, act.collect, (2,)),
+        (ALL, act.collect, (3,)),
+    ]
+
+
+def nearest_first(chips):
+    def key(z):
+        return lambda k: (abs(k - z), abs(2 * k - (chips - 1)))
+
+    return [sorted((k for k in range(chips) if k != z), key=key(z)) for z in range(chips)]
 
 
 def silu(value):
@@ -176,26 +235,38 @@
 
 def fused_kernel(
     shape,
-    outer_ref,
-    inner_ref,
-    value_ref,
-    taps_ref,
+    outer_hbm,
+    inner_hbm,
+    value_hbm,
+    taps_hbm,
     mix_hbm,
-    gain_m_ref,
-    bias_m_ref,
-    moe_ref,
-    ids_ref,
-    route_w_ref,
+    gain_m_hbm,
+    bias_m_hbm,
+    moe_hbm,
+    ids_hbm,
+    route_w_hbm,
     gate_hbm,
     up_hbm,
     down_hbm,
     shared_gate_hbm,
     shared_up_hbm,
     shared_down_hbm,
+    gain_e_hbm,
+    bias_e_hbm,
+    out_m_hbm,
+    out_e_hbm,
+    out_m_ref,
+    out_e_ref,
+    outer_ref,
+    inner_ref,
+    value_ref,
+    taps_ref,
+    ids_ref,
+    route_w_ref,
+    gain_m_ref,
+    bias_m_ref,
     gain_e_ref,
     bias_e_ref,
-    out_m_ref,
-    out_e_ref,
     mix_v,
     gate_v,
     up_v,
@@ -221,8 +292,12 @@
     mixed_ref,
     total_ref,
     load_sem,
+    out_sem,
     send_sem,
     recv_sem,
+    line_recv,
+    route_recv,
+    return_recv,
 ):
     ep_count, tp_count, capacity, seq_length = shape
     chips = ep_count // CORES
@@ -240,108 +315,165 @@
     other = z * CORES + (1 - c)
     f32, bf16 = jnp.float32, jnp.bfloat16
 
-    order = (
-        (shared_gate_hbm, shared_gate_v),
-        (shared_up_hbm, shared_up_v),
-        (gate_hbm.at[0], gate_v),
-        (up_hbm.at[0], up_v),
-        (mix_hbm, mix_v),
-        (down_hbm.at[0], down_v),
-        (shared_down_hbm, shared_down_v),
-    )
-    loads = [pltpu.make_async_copy(a, b, load_sem.at[n]) for n, (a, b) in enumerate(order)]
-    for load in loads:
-        load.start()
-
+    orders = nearest_first(chips)
+
+    def pick(values):
+        chosen = jnp.int32(values[0])
+        for k in range(1, chips):
+            chosen = jnp.where(z == k, values[k], chosen)
+        return chosen
+
+    sources = [z] + [pick([orders[k][s - 1] for k in range(chips)]) for s in range(1, chips)]
+
+    def onward_of(k, s):
+        q = orders[k][s - 1]
+        n = k + 1 if q < k else k - 1
+        there = 0 <= n < chips
+        return n if there else k, there, there and orders[n].index(q) + 1 in WHOLE
+
+    stores = (
+        pltpu.make_async_copy(out_m_ref, out_m_hbm, out_sem.at[0]),
+        pltpu.make_async_copy(out_e_ref, out_e_hbm, out_sem.at[1]),
+    )
+    loads = []
+
+    def load(source, target):
+        loads.append(pltpu.make_async_copy(source, target, load_sem.at[len(loads)]))
+        loads[-1].start()
+        return loads[-1]
+
+    barrier = pltpu.get_barrier_semaphore()
+    for step in range(1, ep_count):
+        pl.semaphore_signal(barrier, inc=1, device_id=((me + step) % ep_count, j), device_id_type=pl.DeviceIdType.MESH)
+    for peer in (jx, jy, jd):
+        pl.semaphore_signal(barrier, inc=1, device_id=(me, peer), device_id_type=pl.DeviceIdType.MESH)
+
+    moe_load = load(moe_hbm, tokens.at[z, 0])
+    ids_load = load(ids_hbm, ids_ref)
+    route_w_load = load(route_w_hbm, route_w_ref)
+    inner_load = load(inner_hbm, inner_ref)
+    value_load = load(value_hbm, value_ref)
+    shared_gate_load = load(shared_gate_hbm, shared_gate_v)
+    shared_up_load = load(shared_up_hbm, shared_up_v)
+    gate_load = load(gate_hbm.at[0], gate_v)
+    up_load = load(up_hbm.at[0], up_v)
+    outer_load = load(outer_hbm, outer_ref)
+    taps_load = load(taps_hbm, taps_ref)
+    gain_m_load = load(gain_m_hbm, gain_m_ref)
+    bias_m_load = load(bias_m_hbm, bias_m_ref)
+    gain_e_load = load(gain_e_hbm, gain_e_ref)
+    bias_e_load = load(bias_e_hbm, bias_e_ref)
+    shared_down_load = load(shared_down_hbm, shared_down_v)
+    down_load = load(down_hbm.at[0], down_v)
+    mix_load = load(mix_hbm, mix_v)
+
+    def loaded(*several):
+        for one in several:
+            one.wait()
+
+    loaded(ids_load, route_w_load)
+    named = lax.broadcasted_iota(jnp.int32, (ep_count, rows), 0)
+    dense = jnp.zeros((ep_count, rows), f32)
+    for k in range(ids_ref.shape[0]):
+        dense = dense + jnp.where(named == ids_ref[k : k + 1, :], route_w_ref[k : k + 1, :], 0.0)
+    route[z, 0] = dense
+    loaded(inner_load, value_load)
     product = (inner_ref[...].astype(f32) * value_ref[...].astype(f32)).astype(bf16)
     edge_rows = edge.shape[0]
     edge[...] = product[rows - edge_rows :]
     pad = extended.shape[0] - rows
     extended[pad:, :] = product.astype(f32)
-    named = lax.broadcasted_iota(jnp.int32, (ep_count, rows), 0)
-    dense = jnp.zeros((ep_count, rows), f32)
-    for k in range(ids_ref.shape[0]):
-        dense = dense + jnp.where(named == ids_ref[k : k + 1, :], route_w_ref[k : k + 1, :], 0.0)
-    route[0, 0] = dense
-
-    barrier = pltpu.get_barrier_semaphore()
-    for step in range(1, ep_count):
-        pl.semaphore_signal(barrier, inc=1, device_id=((me + step) % ep_count, j), device_id_type=pl.DeviceIdType.MESH)
-    for peer in (jx, jy, jd):
-        pl.semaphore_signal(barrier, inc=1, device_id=(me, peer), device_id_type=pl.DeviceIdType.MESH)
-    pl.semaphore_wait(barrier, ep_count - 1 + tp_count - 1)
-
+    loaded(moe_load)
+
+    with jax.named_scope("barrier"):
+        pl.semaphore_wait(barrier, ep_count - 1 + tp_count - 1)
+
+    groups = {}
     numbers = {}
-    started = []
-
-    def number(name):
-        return numbers.setdefault(name, len(numbers))
-
-    def copy(name, source, target, device):
-        n = number(name)
+
+    def remote(source, target, sent, received, device):
         return pltpu.make_async_remote_copy(
             src_ref=source,
             dst_ref=target,
-            send_sem=send_sem.at[n],
-            recv_sem=recv_sem.at[n],
+            send_sem=sent,
+            recv_sem=received,
             device_id=device,
             device_id_type=pl.DeviceIdType.MESH,
         )
 
-    def send(name, source, target, device):
-        c_ = copy(name, source, target, device)
-        c_.start()
-        started.append(c_)
-
-    def arrive(name, target):
-        copy(name, target, target, (other, j)).wait_recv()
+    def group(name):
+        return send_sem.at[groups.setdefault(name, len(groups))]
+
+    def number(name):
+        return recv_sem.at[numbers.setdefault(name, len(numbers))]
+
+    def send(many, name, source, target, device, received=None, when=None):
+        copy = remote(source, target, group(many), number(name) if received is None else received, device)
+        if when is None:
+            copy.start()
+        else:
+            pl.when(when)(copy.start)
+
+    def arrive(name, target, received=None):
+        remote(target, target, group(EDGE), number(name) if received is None else received, (other, j)).wait_recv()
+
+    def sent(many, ref, when=None):
+        def wait():
+            remote(ref, ref, group(many), number(EDGE), (other, j)).wait_send()
+
+        if when is None:
+            wait()
+        else:
+            pl.when(when)(wait)
 
     def columns(owner):
         return pl.ds(pl.multiple_of(owner * cols, cols), cols)
 
-    def gather_start(name, ref):
+    def gather_x(name, ref):
         part = ref.at[:, columns(j)]
-        send(name + ("x",), part, part, (me, jx))
-        send(name + ("y",), part, part, (me, jy))
-
-    def gather_relay(name, ref):
+        send(name[0], name + (0,), part, part, (me, jx))
+
+    def gather_y(name, ref):
+        part = ref.at[:, columns(j)]
+        send(name[0], name + (1,), part, part, (me, jy))
+
+    def relay_x(name, ref):
         half = ref.shape[0] // 2
-        arrive(name + ("x",), ref.at[:, columns(jx)])
+        arrive(name + (0,), ref.at[:, columns(jx)])
         part = ref.at[pl.ds(0, half), columns(jx)]
-        send(name + ("xy",), part, part, (me, jy))
-        arrive(name + ("y",), ref.at[:, columns(jy)])
+        send(name[0], name + (2,), part, part, (me, jy))
+
+    def relay_y(name, ref):
+        half = ref.shape[0] // 2
+        arrive(name + (1,), ref.at[:, columns(jy)])
         part = ref.at[pl.ds(half, half), columns(jy)]
-        send(name + ("yx",), part, part, (me, jx))
+        send(name[0], name + (2,), part, part, (me, jx))
 
     def gather_finish(name, ref):
-        half = ref.shape[0] // 2
-        arrive(name + ("xy",), ref.at[pl.ds(0, half), columns(jd)])
-        arrive(name + ("yx",), ref.at[pl.ds(half, half), columns(jd)])
-
-    send(("pair", 0), moe_ref, tokens.at[0, 1], (other, j))
-    for s in range(chips):
-        target = (z - s + chips) % chips
-        if s > 0:
-            send(("route", s, 0), route.at[0, 0], route.at[s, 0], (target * CORES + c, j))
-        send(("route", s, 1), route.at[0, 0], route.at[s, 1], (target * CORES + (1 - c), j))
+        arrive(name + (2,), ref.at[:, columns(jd)])
+
+    above = (z + 1) % chips
+    below = (z + chips - 1) % chips
+    quarters = (x, PLANE + y, 1 - x, PLANE + 1 - y)
+    for k, quarter in enumerate(quarters[:PLANE]):
+        part = tokens.at[z, 0, :, columns(quarter)]
+        received = line_recv.at[z, k]
+        send(UP, (), part, part, (above * CORES + c, j), received, z + 1 < chips)
+        send(DOWN, (), part, part, (below * CORES + c, j), received, z > 0)
+    send(NEAR, (), route.at[z, 0], route.at[z, 1], (other, j), route_recv.at[z])
+    send(PAIR, (PAIR, 0), tokens.at[z, 0], tokens.at[z, 1], (other, j))
     for s in range(1, chips):
-        target = (z - s + chips) % chips
-        send(
-            ("line", s),
-            moe_ref.at[:, columns(j)],
-            tokens.at[s, 0, :, columns(j)],
-            (target * CORES + c, j),
-        )
-    send(("edge",), edge, border, ((me + 1) % ep_count, j))
+        target = (z + s) % chips
+        for p in range(CORES):
+            device = (target * CORES + (c if p == 0 else 1 - c), j)
+            send(ROUTE, (), route.at[z, 0], route.at[z, p], device, route_recv.at[z])
+    send(EDGE, EDGE, edge, border, ((me + 1) % ep_count, j))
 
     def dot(a, b):
         return jnp.dot(a, b, preferred_element_type=f32)
 
-    def token_ref(s, p):
-        return moe_ref if (s, p) == (0, 0) else tokens.at[s, p]
-
     def choice(s, p):
-        weight = route[s, p, pl.ds(me, 1), :]
+        weight = route[sources[s], p, pl.ds(me, 1), :]
         routed = (weight > 0.0).astype(f32)
         earlier = lax.broadcasted_iota(jnp.int32, (rows, rows), 0)
         later = lax.broadcasted_iota(jnp.int32, (rows, rows), 1)
@@ -351,30 +483,127 @@
         slot = lax.broadcasted_iota(jnp.int32, (capacity, rows), 0).astype(f32) + 1.0
         return (slot == rank).astype(f32), weight
 
-    def expert_up_stage(s):
+    def line_arrival(s, k):
+        q = sources[s]
+        quarter = quarters[k]
+        part = tokens.at[q, 0, :, columns(quarter)]
+        arrive((), part, line_recv.at[q, k])
+        onward_send(s, k)
+        if s not in WHOLE:
+            send(CROSS, (CROSS, s, k), part, part, (me, (jx, jy)[k]))
+        send(PAIR, (PAIR, s), part, tokens.at[q, 1, :, columns(quarter)], (other, j))
+
+    onwards = {}
+    for s in range(1, chips):
+        for k in range(tp_count):
+            told = [onward_of(n, s)[1 if k < PLANE else 2] for n in range(chips)]
+            if any(told):
+                onward = pick([onward_of(n, s)[0] for n in range(chips)])
+                onwards[s, k] = (onward, pick([int(t) for t in told]) > 0)
+
+    def onward_send(s, k):
+        q = sources[s]
+        part = tokens.at[q, 0, :, columns(quarters[k])]
+        if (s, k) in onwards:
+            onward, more = onwards[s, k]
+            device = (onward * CORES + c, j)
+            send((ONWARD, s, k - k % PLANE), (), part, part, device, line_recv.at[q, k], more)
+
+    def cross_arrival(s, k):
+        if s in WHOLE:
+            line_arrival(s, k)
+            return
+        q = sources[s]
+        part = tokens.at[q, 0, :, columns(quarters[k])]
+        arrive((CROSS, s, k - PLANE), part)
+        onward_send(s, k)
+        send(PAIR, (PAIR, s), part, tokens.at[q, 1, :, columns(quarters[k])], (other, j))
+
+    def expert_up(s):
+        q = sources[s]
+        arrive((), route.at[q] if s else route.at[q, 1], route_recv.at[q])
+        if s == 0:
+            loaded(gate_load, up_load)
         for p in range(CORES):
             picks, _ = choice(s, p)
+            if p == 1:
+                arrive((PAIR, s), tokens.at[q, 1])
             rows_in[p * capacity : (p + 1) * capacity, :] = dot(
-                picks.astype(bf16), token_ref(s, p)[...]
+                picks.astype(bf16), tokens[q, p]
             ).astype(bf16)
         held = silu(dot(rows_in[...], gate_v[...])) * dot(rows_in[...], up_v[...])
-        hidden[s, :, columns(j)] = held.astype(bf16)
-
-    def hidden_start(s):
-        gather_start(("hidden", s), hidden.at[s])
-
-    def hidden_relay(s):
-        gather_relay(("hidden", s), hidden.at[s])
-
-    def token_relay(s):
-        gather_relay(("tokens", s), tokens.at[s, 0])
+        hidden[q, :, columns(j)] = held.astype(bf16)
+
+    def up_part(s, t):
+        q = sources[s]
+        p = (t + c) % CORES
+        if t == 0:
+            arrive((), route.at[q], route_recv.at[q])
+            arrive((PAIR, s), tokens.at[q, 1])
+        picks, _ = choice(s, p)
+        taken = dot(picks.astype(bf16), tokens[q, p]).astype(bf16)
+        held = silu(dot(taken, gate_v[...])) * dot(taken, up_v[...])
+        hidden[q, t * capacity : (t + 1) * capacity, columns(j)] = held.astype(bf16)
+
+    def part_ref(s, t):
+        return hidden.at[sources[s], pl.ds(t * capacity, capacity)]
+
+    def down_part(s, t):
+        q = sources[s]
+        gather_finish((HIDDEN, s, t), part_ref(s, t))
+        picks, weight = choice(s, (t + c) % CORES)
+        full = dot(hidden[q, t * capacity : (t + 1) * capacity], down_v[...])
+        scale = jnp.sum(picks * weight, axis=1, keepdims=True)
+        scaled = (full * scale).astype(bf16)
+        spread = lax.dot_general(
+            picks.astype(bf16), scaled, (((0,), (0,)), ((), ())), preferred_element_type=f32
+        ).astype(bf16)
+
+        @pl.when(c == t)
+        def _():
+            sent_sum[q] = spread
+
+        @pl.when(c != t)
+        def _():
+            own_part[q] = spread
+            send(PART, (PART, s), own_part.at[q], peer_part.at[q], (other, j))
+
+    def return_part(s, t):
+        @pl.when(c == t)
+        def _():
+            expert_return(s)
+
+    def start_x(s):
+        gather_x((HIDDEN, s), hidden.at[sources[s]])
+
+    def start_y(s):
+        gather_y((HIDDEN, s), hidden.at[sources[s]])
+
+    def start(s):
+        start_x(s)
+        start_y(s)
+
+    def relay(s):
+        relay_x((HIDDEN, s), hidden.at[sources[s]])
+        relay_y((HIDDEN, s), hidden.at[sources[s]])
+
+    def start_part(s, t):
+        gather_x((HIDDEN, s, t), part_ref(s, t))
+        gather_y((HIDDEN, s, t), part_ref(s, t))
+
+    def relay_part(s, t):
+        relay_x((HIDDEN, s, t), part_ref(s, t))
+        relay_y((HIDDEN, s, t), part_ref(s, t))
 
     def collect(s):
-        arrive(("return", s), returned.at[s])
-        total_ref[...] = total_ref[...] + returned[s].astype(f32)
-
-    def expert_down_stage(s):
-        full = dot(hidden[s], down_v[...])
+        q = sources[s]
+        arrive((), returned.at[q], return_recv.at[q])
+        total_ref[...] = total_ref[...] + returned[q].astype(f32)
+
+    def expert_down(s):
+        q = sources[s]
+        gather_finish((HIDDEN, s), hidden.at[q])
+        full = dot(hidden[q], down_v[...])
         for p in reversed(range(CORES)):
             picks, weight = choice(s, p)
             scale = jnp.sum(picks * weight, axis=1, keepdims=True)
@@ -383,34 +612,21 @@
                 picks.astype(bf16), scaled, (((0,), (0,)), ((), ())), preferred_element_type=f32
             )
             if p == 1:
-                own_part[s] = spread.astype(bf16)
-                send(("part", s), own_part.at[s], peer_part.at[s], (other, j))
+                own_part[q] = spread.astype(bf16)
+                send(PART, (PART, s), own_part.at[q], peer_part.at[q], (other, j))
             elif s == 0:
                 total_ref[...] = total_ref[...] + spread
             else:
-                sent_sum[s] = spread.astype(bf16)
+                sent_sum[q] = spread.astype(bf16)
 
     def expert_return(s):
-        arrive(("part", s), peer_part.at[s])
+        q = sources[s]
+        arrive((PART, s), peer_part.at[q])
         if s == 0:
-            total_ref[...] = total_ref[...] + peer_part[0].astype(f32)
+            total_ref[...] = total_ref[...] + peer_part[q].astype(f32)
         else:
-            sent_sum[s] = (sent_sum[s].astype(f32) + peer_part[s].astype(f32)).astype(bf16)
-            target = (z + s) % chips
-            send(("return", s), sent_sum.at[s], returned.at[s], (target * CORES + c, j))
-
-    def wait_routes(s):
-        for p in range(CORES):
-            if (s, p) != (0, 0):
-                arrive(("route", s, p), route.at[s, p])
-
-    def pair_tokens(s):
-        gather_finish(("tokens", s), tokens.at[s, 0])
-        send(("pair", s), tokens.at[s, 0], tokens.at[s, 1], (other, j))
-
-    def line_tokens(s):
-        arrive(("line", s), tokens.at[s, 0, :, columns(j)])
-        gather_start(("tokens", s), tokens.at[s, 0])
+            sent_sum[q] = (sent_sum[q].astype(f32) + peer_part[q].astype(f32)).astype(bf16)
+            send(RETURN, (), sent_sum.at[q], returned.at[z], (q * CORES + c, j), return_recv.at[z])
 
     def stats_start(k, values):
         lane = lax.broadcasted_iota(jnp.int32, (rows, rows), 1)
@@ -419,12 +635,12 @@
         tile = jnp.where(lane == 0, total, jnp.where(lane == 1, square, 0.0))
         stats_out[k] = tile.T[0 : stats_out.shape[1], :]
         for n, peer in enumerate((jx, jy, jd)):
-            send(("stats", k, n), stats_out.at[k], stats_in.at[k, n], (me, peer))
+            send((STATS, k), (STATS, k), stats_out.at[k], stats_in.at[k, n], (me, peer))
 
     def stats_finish(k, values, gain_ref, bias_ref, out_ref):
         tile = stats_out[k]
+        arrive((STATS, k), stats_in.at[k])
         for n in range(tp_count - 1):
-            arrive(("stats", k, n), stats_in.at[k, n])
             tile = tile + stats_in[k, n]
         padded = jnp.concatenate(
             [tile, jnp.zeros((rows - tile.shape[0], rows), f32)], axis=0
@@ -437,15 +653,17 @@
             + bias_ref[...].astype(f32).reshape(1, cols)
         ).astype(bf16)
 
-    def shared_start(_):
-        loads[0].wait()
-        loads[1].wait()
-        held = silu(dot(moe_ref[...], shared_gate_v[...])) * dot(moe_ref[...], shared_up_v[...])
+    def shared_start():
+        loaded(shared_gate_load, shared_up_load)
+        own = tokens[z, 0]
+        held = silu(dot(own, shared_gate_v[...])) * dot(own, shared_up_v[...])
         shared_hidden[:, columns(j)] = held.astype(bf16)
-        gather_start(("shared",), shared_hidden)
-
-    def mixer_start(_):
-        arrive(("edge",), border)
+        gather_x((SHARED,), shared_hidden)
+        gather_y((SHARED,), shared_hidden)
+
+    def mixer_start():
+        arrive(EDGE, border)
+        loaded(outer_load, taps_load)
         extended[pad - edge_rows : pad, :] = border[...].astype(f32)
         places = (me * rows + lax.broadcasted_iota(jnp.int32, (rows, 1), 0)) % seq_length
         taps_count = taps_ref.shape[0]
@@ -456,65 +674,92 @@
             kept = (places >= delay).astype(f32)
             convolved = convolved + taps_ref[offset : offset + 1, :].astype(f32) * delayed * kept
         weighted[:, columns(j)] = (outer_ref[...].astype(f32) * convolved).astype(bf16)
-        gather_start(("mixer",), weighted)
-
-    def expert_up_start(s):
-        wait_routes(s)
-        arrive(("pair", s), tokens.at[s, 1])
-        if s == 0:
-            loads[2].wait()
-            loads[3].wait()
-        expert_up_stage(s)
-
-    def shared_relay(_):
-        gather_relay(("shared",), shared_hidden)
-
-    def mixer_relay(_):
-        gather_relay(("mixer",), weighted)
-
-    def mixer_dot(_):
-        gather_finish(("mixer",), weighted)
-        loads[4].wait()
+        gather_x((MIXER,), weighted)
+        gather_y((MIXER,), weighted)
+
+    def shared_relay():
+        relay_x((SHARED,), shared_hidden)
+        relay_y((SHARED,), shared_hidden)
+
+    def mixer_relay():
+        relay_x((MIXER,), weighted)
+        relay_y((MIXER,), weighted)
+
+    def mixer_dot():
+        gather_finish((MIXER,), weighted)
+        loaded(mix_load)
         mixed_ref[...] = dot(weighted[...], mix_v[...])
         stats_start(0, mixed_ref[...])
 
-    def mixer_end(_):
+    def mixer_end():
+        loaded(gain_m_load, bias_m_load, gain_e_load, bias_e_load)
         stats_finish(0, mixed_ref[...], gain_m_ref, bias_m_ref, out_m_ref)
-
-    def shared_dot(_):
-        gather_finish(("shared",), shared_hidden)
-        loads[6].wait()
+        stores[0].start()
+
+    def shared_dot():
+        gather_finish((SHARED,), shared_hidden)
+        loaded(shared_down_load, down_load)
         total_ref[...] = dot(shared_hidden[...], shared_down_v[...])
-        loads[5].wait()
-
-    def expert_down(s):
-        gather_finish(("hidden", s), hidden.at[s])
-        expert_down_stage(s)
-
-    acts = {
-        "shared": shared_start,
-        "mixer": mixer_start,
-        "shared_relay": shared_relay,
-        "mixer_relay": mixer_relay,
-        "mixer_dot": mixer_dot,
-        "mixer_end": mixer_end,
-        "shared_dot": shared_dot,
-        "line": line_tokens,
-        "token_relay": token_relay,
-        "pair": pair_tokens,
-        "up": expert_up_start,
-        "hidden": hidden_start,
-        "hidden_relay": hidden_relay,
-        "down": expert_down,
-        "return": expert_return,
-        "collect": collect,
-    }
-    for act, s in plan(chips):
-        acts[act](s)
-    stats_start(1, total_ref[...])
-    stats_finish(1, total_ref[...], gain_e_ref, bias_e_ref, out_e_ref)
-    for item in started:
-        item.wait_send()
+
+    act = types.SimpleNamespace(
+        shared=shared_start,
+        up=expert_up,
+        start=start,
+        start_x=start_x,
+        start_y=start_y,
+        line=line_arrival,
+        cross=cross_arrival,
+        relay=relay,
+        down=expert_down,
+        give_back=expert_return,
+        up_part=up_part,
+        start_part=start_part,
+        relay_part=relay_part,
+        down_part=down_part,
+        give_back_part=return_part,
+        shared_relay=shared_relay,
+        shared_dot=shared_dot,
+        mixer=mixer_start,
+        mixer_relay=mixer_relay,
+        mixer_dot=mixer_dot,
+        collect=collect,
+    )
+    inner = (z > 0) & (z < chips - 1)
+    for where, step, which in plan(act):
+        if where == ALL:
+            step(*which)
+        else:
+            pl.when(inner if where == INNER else ~inner)(functools.partial(step, *which))
+    with jax.named_scope("stats"):
+        stats_start(1, total_ref[...])
+    with jax.named_scope("mixer_end"):
+        mixer_end()
+    with jax.named_scope("drain"):
+        lines = tokens.at[0, 0, :, pl.ds(0, PLANE * cols)]
+        sent(UP, lines, z + 1 < chips)
+        sent(DOWN, lines, z > 0)
+        for s, k in onwards:
+            if k % PLANE == 0:
+                sent((ONWARD, s, k), lines, onwards[s, k][1])
+        sent(NEAR, route.at[0, 0])
+        sent(PAIR, tokens.at[:, 0])
+        sent(ROUTE, route.at[pl.ds(0, chips - 1)])
+        sent(EDGE, edge)
+        sent(CROSS, tokens.at[pl.ds(0, chips - 1 - len(WHOLE)), 0, :, pl.ds(0, PLANE * cols)])
+        gathered = pl.ds(0, (tp_count - 1) * cols)
+        sent(HIDDEN, hidden.at[:, :, gathered])
+        sent(SHARED, shared_hidden.at[:, gathered])
+        sent(MIXER, weighted.at[:, gathered])
+        sent(PART, own_part)
+        sent(RETURN, own_part.at[pl.ds(0, chips - 1)])
+        sent((STATS, 0), stats_in.at[0])
+    with jax.named_scope("finish"):
+        stats_finish(1, total_ref[...], gain_e_ref, bias_e_ref, out_e_ref)
+    stores[1].start()
+    with jax.named_scope("sent"):
+        sent((STATS, 1), stats_in.at[1])
+        for store in stores:
+            store.wait()
 
 
 def pass_kernel(first_ref, second_ref, out_first_ref, out_second_ref):
@@ -552,9 +797,14 @@
     bf16, f32 = jnp.bfloat16, jnp.float32
     vmem = pl.BlockSpec(memory_space=pltpu.VMEM)
     hbm = pl.BlockSpec(memory_space=pl.ANY)
-    copies = 16 * chips + 24
+    copies = 4 * chips + 20
     weight = pltpu.VMEM((width, cols), bf16)
     scratch = [
+        *([pltpu.VMEM((rows, cols), bf16)] * 5),
+        pltpu.VMEM(conv_taps.shape, bf16),
+        pltpu.VMEM(route_ids.shape[::-1], jnp.int32),
+        pltpu.VMEM(route_weights.shape[::-1], f32),
+        *([pltpu.VMEM((cols,), bf16)] * 4),
         *([weight] * 7),
         pltpu.VMEM((chips, CORES, rows, width), bf16),
         pltpu.VMEM((chips, CORES, ep_count, rows), f32),
@@ -573,18 +823,20 @@
         pltpu.VMEM((2, tp_count - 1, 8, rows), f32),
         pltpu.VMEM((rows, cols), f32),
         pltpu.VMEM((rows, cols), f32),
-        pltpu.SemaphoreType.DMA((7,)),
+        pltpu.SemaphoreType.DMA((18,)),
+        pltpu.SemaphoreType.DMA((2,)),
+        pltpu.SemaphoreType.DMA((chips + 15,)),
         pltpu.SemaphoreType.DMA((copies,)),
-        pltpu.SemaphoreType.DMA((copies,)),
+        pltpu.SemaphoreType.DMA((chips, tp_count)),
+        pltpu.SemaphoreType.DMA((chips,)),
+        pltpu.SemaphoreType.DMA((chips,)),
     ]
     out = jax.ShapeDtypeStruct((rows, cols), bf16)
     first, second = pl.pallas_call(
         functools.partial(fused_kernel, (ep_count, tp_count, capacity, seq_length)),
         out_shape=(out, out),
-        in_specs=[vmem] * 4 + [hbm] + [vmem] * 5
-        + [hbm] * 6
-        + [vmem, vmem],
-        out_specs=(vmem, vmem),
+        in_specs=[hbm] * 18,
+        out_specs=(hbm, hbm),
         scratch_shapes=scratch,
         compiler_params=pltpu.CompilerParams(
             collective_id=0, has_side_effects=True, vmem_limit_bytes=VMEM_BYTES
@@ -617,7 +869,7 @@
 def on_device(*arrays):
     local_experts = arrays[10].shape[0]
     square = lax.axis_size("tp") == PLANE * PLANE
-    if square and local_experts == 1 and lax.axis_size("ep") % CORES == 0:
+    if square and local_experts == 1 and lax.axis_size("ep") == CORES * LINE:
         return fused_device(*arrays)
     return plain_device(*arrays)
 

time: 74.6 us -> 60.7 us (0.81)
  Pallas kernels: 73.5 us -> 59.9 us
    pallas_call x1, Pallas kernels: 71.8 us -> 58.2 us  [fused_device(): pl.pallas_call(functools.partial(fused_kernel, (ep_count, tp_count, capac...]
where the time goes in v1:
time: 60.7 us; the launch traced here: 60.5 us
  Pallas kernels  59.9 us (99%)
  between operations  0.65 us (1%)
    pallas_call x1, Pallas kernels, fused_device(): pl.pallas_call(functools.partial(fused_kernel, (ep_count, tp_count, capac...  58.2 us
    pallas_call x1, Pallas kernels, fused_device(): pl.pallas_call(pass_kernel, out_shape=(out, out), in_specs=[vmem, vmem],...  1.68 us

profile of v1, /device:TPU:0, one launch (start us, length us, event | category | flops | bytes accessed | tf_op | source)
XLA Modules:
  0.0 60.5 jit_solution(9759794962060146058)
XLA Ops:
  0.6 58.2 %shard_map.185 = (bf16[128,512]{1,0:T(8,128)(2,1)}, bf16[128,512]{1,0:T(8,128)(2,1)}) custom-call(bf16[128,512]{1,0:T(8,128)(2,1)} %outer_hbm.1, bf16[128,512]{1,0:T(8,128)(2,1)} %inner_hbm.1, bf16[128,512]{1,0:T(8,128)(2,1)} %value_hbm.1, bf16[3,512]{1,0:T(4,128)(2,1)} %taps_hbm.1, bf16[2048,512]{1,0:T(8,128)(2,1)} %mix_hbm.1, bf16[512]{0:T(512)(128)(2,1)} %gain_m_hbm.1, ...), custom_call_target="tpu_custom_call" | custom-call | tf_op jit(solution)/shard_map/pallas_call | solution.py:835
  58.9 1.7 %shard_map.186 = (bf16[128,512]{1,0:T(8,128)(2,1)}, bf16[128,512]{1,0:T(8,128)(2,1)}) custom-call(bf16[128,512]{1,0:T(8,128)(2,1)} %get-tuple-element.4.first_ref, bf16[128,512]{1,0:T(8,128)(2,1)} %get-tuple-element.5.second_ref), custom_call_target="tpu_custom_call" | custom-call | tf_op jit(solution)/shard_map/pallas_call | solution.py:864

commit v2 on v1

--- a/solution.py
+++ b/solution.py
@@ -137,14 +137,14 @@
 
 
 PLANE = 2
+SMALL_BYTES = 4 * 1024 * 1024
 CORES = 2
-VMEM_BYTES = 60 * 1024 * 1024
+VMEM_BYTES = 48 * 1024 * 1024
 
 
 (
     UP,
     DOWN,
-    NEAR,
     ROUTE,
     PAIR,
     EDGE,
@@ -156,9 +156,10 @@
     RETURN,
     STATS,
     ONWARD,
-) = range(14)
+    ROUTE_UP,
+    ROUTE_DOWN,
+) = range(15)
 LINE = 4
-WHOLE = (3,)
 ALL, INNER, OUTER = range(3)
 
 
@@ -167,51 +168,58 @@
         (ALL, act.shared, ()),
         (ALL, act.up, (0,)),
         (ALL, act.start_y, (0,)),
-        (ALL, act.line, (1, 0)),
+        (ALL, act.line, (1, 0, True)),
         (INNER, act.line, (2, 0)),
         (ALL, act.start_x, (0,)),
-        (ALL, act.line, (1, 1)),
+        (ALL, act.line, (1, 1, True)),
         (INNER, act.line, (2, 1)),
-        (OUTER, act.line, (2, 0)),
+        (OUTER, act.line, (2, 0, True)),
+        (INNER, act.line, (2, 2)),
         (INNER, act.line, (3, 0)),
         (ALL, act.cross, (1, 2)),
         (ALL, act.cross, (1, 3)),
-        (OUTER, act.line, (2, 1)),
+        (INNER, act.line, (2, 3)),
+        (OUTER, act.line, (2, 1, True)),
         (INNER, act.line, (3, 1)),
-        (INNER, act.cross, (2, 2)),
         (ALL, act.shared_relay, ()),
         (ALL, act.up, (1,)),
         (ALL, act.start, (1,)),
-        (INNER, act.cross, (2, 3)),
+        (INNER, act.line, (3, 2)),
         (OUTER, act.line, (3, 0)),
         (OUTER, act.cross, (2, 2)),
-        (INNER, act.cross, (3, 2)),
         (OUTER, act.cross, (2, 3)),
         (OUTER, act.line, (3, 1)),
+        (OUTER, act.relay, (0,)),
         (ALL, act.up, (2,)),
         (ALL, act.start, (2,)),
-        (INNER, act.cross, (3, 3)),
-        (ALL, act.relay, (1,)),
+        (INNER, act.line, (3, 3)),
         (ALL, act.shared_dot, ()),
-        (OUTER, act.cross, (3, 2)),
-        (OUTER, act.cross, (3, 3)),
+        (OUTER, act.line, (3, 2)),
+        (OUTER, act.line, (3, 3)),
+        (INNER, act.relay, (1,)),
+        (INNER, act.relay, (2,)),
         (ALL, act.up_part, (3, 0)),
         (ALL, act.start_part, (3, 0)),
-        (ALL, act.relay, (2,)),
+        (OUTER, act.relay, (2,)),
         (ALL, act.up_part, (3, 1)),
         (ALL, act.start_part, (3, 1)),
-        (ALL, act.down, (1,)),
-        (ALL, act.give_back, (1,)),
+        (INNER, act.down, (1,)),
+        (INNER, act.give_back, (1,)),
+        (INNER, act.down, (2,)),
         (ALL, act.relay_part, (3, 0)),
-        (ALL, act.down, (2,)),
+        (INNER, act.give_back, (2,)),
+        (OUTER, act.down, (2,)),
         (ALL, act.relay_part, (3, 1)),
-        (ALL, act.give_back, (2,)),
+        (OUTER, act.relay, (1,)),
+        (OUTER, act.give_back, (2,)),
         (ALL, act.mixer, ()),
-        (ALL, act.relay, (0,)),
+        (INNER, act.relay, (0,)),
         (ALL, act.down_part, (3, 0)),
         (ALL, act.give_back_part, (3, 0)),
         (ALL, act.down_part, (3, 1)),
         (ALL, act.give_back_part, (3, 1)),
+        (OUTER, act.down, (1,)),
+        (OUTER, act.give_back, (1,)),
         (ALL, act.mixer_relay, ()),
         (ALL, act.down, (0,)),
         (ALL, act.give_back, (0,)),
@@ -253,8 +261,6 @@
     shared_down_hbm,
     gain_e_hbm,
     bias_e_hbm,
-    out_m_hbm,
-    out_e_hbm,
     out_m_ref,
     out_e_ref,
     outer_ref,
@@ -292,7 +298,6 @@
     mixed_ref,
     total_ref,
     load_sem,
-    out_sem,
     send_sem,
     recv_sem,
     line_recv,
@@ -325,16 +330,19 @@
 
     sources = [z] + [pick([orders[k][s - 1] for k in range(chips)]) for s in range(1, chips)]
 
+    def whole(k, q):
+        s = orders[k].index(q) + 1
+        return s == chips - 1 or s == chips - 2 and 0 < k < chips - 1
+
     def onward_of(k, s):
         q = orders[k][s - 1]
         n = k + 1 if q < k else k - 1
         there = 0 <= n < chips
-        return n if there else k, there, there and orders[n].index(q) + 1 in WHOLE
-
-    stores = (
-        pltpu.make_async_copy(out_m_ref, out_m_hbm, out_sem.at[0]),
-        pltpu.make_async_copy(out_e_ref, out_e_hbm, out_sem.at[1]),
-    )
+        return n if there else k, there, there and whole(n, q)
+
+    rising = pick([int(k + 1 < chips and whole(k + 1, k)) for k in range(chips)]) > 0
+    falling = pick([int(k > 0 and whole(k - 1, k)) for k in range(chips)]) > 0
+
     loads = []
 
     def load(source, target):
@@ -342,11 +350,27 @@
         loads[-1].start()
         return loads[-1]
 
+    above = (z + 1) % chips
+    below = (z + chips - 1) % chips
+    higher = z + 1 < chips
+    lower = z > 0
+    beside = jnp.where(c > 0, me + 1, me + ep_count - 1) % ep_count
+    slanted = jnp.where(c > 0, z + 1 < chips, z > 0)
+
     barrier = pltpu.get_barrier_semaphore()
-    for step in range(1, ep_count):
-        pl.semaphore_signal(barrier, inc=1, device_id=((me + step) % ep_count, j), device_id_type=pl.DeviceIdType.MESH)
-    for peer in (jx, jy, jd):
-        pl.semaphore_signal(barrier, inc=1, device_id=(me, peer), device_id_type=pl.DeviceIdType.MESH)
+
+    def greet(row, column):
+        pl.semaphore_signal(
+            barrier, inc=1, device_id=(row, column), device_id_type=pl.DeviceIdType.MESH
+        )
+
+    greet(other, j)
+    greet(me, jx)
+    greet(me, jy)
+    pl.when(higher)(lambda: greet(above * CORES + c, j))
+    pl.when(lower)(lambda: greet(below * CORES + c, j))
+    pl.when(slanted)(lambda: greet(beside, j))
+    greeted = 3 + higher.astype(jnp.int32) + lower.astype(jnp.int32) + slanted.astype(jnp.int32)
 
     moe_load = load(moe_hbm, tokens.at[z, 0])
     ids_load = load(ids_hbm, ids_ref)
@@ -371,22 +395,9 @@
         for one in several:
             one.wait()
 
-    loaded(ids_load, route_w_load)
-    named = lax.broadcasted_iota(jnp.int32, (ep_count, rows), 0)
-    dense = jnp.zeros((ep_count, rows), f32)
-    for k in range(ids_ref.shape[0]):
-        dense = dense + jnp.where(named == ids_ref[k : k + 1, :], route_w_ref[k : k + 1, :], 0.0)
-    route[z, 0] = dense
-    loaded(inner_load, value_load)
-    product = (inner_ref[...].astype(f32) * value_ref[...].astype(f32)).astype(bf16)
-    edge_rows = edge.shape[0]
-    edge[...] = product[rows - edge_rows :]
-    pad = extended.shape[0] - rows
-    extended[pad:, :] = product.astype(f32)
     loaded(moe_load)
-
     with jax.named_scope("barrier"):
-        pl.semaphore_wait(barrier, ep_count - 1 + tp_count - 1)
+        pl.semaphore_wait(barrier, greeted)
 
     groups = {}
     numbers = {}
@@ -452,22 +463,44 @@
     def gather_finish(name, ref):
         arrive(name + (2,), ref.at[:, columns(jd)])
 
-    above = (z + 1) % chips
-    below = (z + chips - 1) % chips
     quarters = (x, PLANE + y, 1 - x, PLANE + 1 - y)
-    for k, quarter in enumerate(quarters[:PLANE]):
-        part = tokens.at[z, 0, :, columns(quarter)]
+    def line_start(k):
+        part = tokens.at[z, 0, :, columns(quarters[k])]
         received = line_recv.at[z, k]
-        send(UP, (), part, part, (above * CORES + c, j), received, z + 1 < chips)
-        send(DOWN, (), part, part, (below * CORES + c, j), received, z > 0)
-    send(NEAR, (), route.at[z, 0], route.at[z, 1], (other, j), route_recv.at[z])
+        more = k - k % PLANE
+        device = (above * CORES + c, j)
+        send((UP, more), (), part, part, device, received, rising if more else higher)
+        device = (below * CORES + c, j)
+        send((DOWN, more), (), part, part, device, received, falling if more else lower)
+
+    line_start(0)
     send(PAIR, (PAIR, 0), tokens.at[z, 0], tokens.at[z, 1], (other, j))
-    for s in range(1, chips):
-        target = (z + s) % chips
-        for p in range(CORES):
-            device = (target * CORES + (c if p == 0 else 1 - c), j)
-            send(ROUTE, (), route.at[z, 0], route.at[z, p], device, route_recv.at[z])
-    send(EDGE, EDGE, edge, border, ((me + 1) % ep_count, j))
+    loaded(ids_load, route_w_load)
+    named = lax.broadcasted_iota(jnp.int32, (ep_count, rows), 0)
+    dense = jnp.zeros((ep_count, rows), f32)
+    for k in range(ids_ref.shape[0]):
+        dense = dense + jnp.where(named == ids_ref[k : k + 1, :], route_w_ref[k : k + 1, :], 0.0)
+    route[z, 0] = dense
+    own = route.at[z, 0]
+    send(ROUTE_UP, (), own, own, (above * CORES + c, j), route_recv.at[z], higher)
+    send(ROUTE_DOWN, (), own, own, (below * CORES + c, j), route_recv.at[z], lower)
+    send(ROUTE, (ROUTE, 0), own, route.at[z, 1], (other, j))
+    line_start(1)
+    line_start(2)
+    line_start(3)
+    loaded(inner_load, value_load)
+    product = (inner_ref[...].astype(f32) * value_ref[...].astype(f32)).astype(bf16)
+    edge_rows = edge.shape[0]
+    edge[...] = product[rows - edge_rows :]
+
+    @pl.when(me == 0)
+    def _():
+        border[...] = jnp.zeros_like(border)
+
+    pad = extended.shape[0] - rows
+    extended[pad:, :] = product.astype(f32)
+    last = me == ep_count - 1
+    send(EDGE, EDGE, edge, border, ((me + 1) % ep_count, j), None, ~last)
 
     def dot(a, b):
         return jnp.dot(a, b, preferred_element_type=f32)
@@ -483,14 +516,22 @@
         slot = lax.broadcasted_iota(jnp.int32, (capacity, rows), 0).astype(f32) + 1.0
         return (slot == rank).astype(f32), weight
 
-    def line_arrival(s, k):
+    def line_arrival(s, k, swap=False):
         q = sources[s]
         quarter = quarters[k]
         part = tokens.at[q, 0, :, columns(quarter)]
+        if k == 1:
+            own = route.at[q, 0]
+            arrive((), own, route_recv.at[q])
+            if (s, k) in onwards:
+                onward, more = onwards[s, k]
+                device = (onward * CORES + c, j)
+                send((ROUTE, s), (), own, own, device, route_recv.at[q], more)
+            send(ROUTE, (ROUTE, s), own, route.at[q, 1], (other, j))
         arrive((), part, line_recv.at[q, k])
         onward_send(s, k)
-        if s not in WHOLE:
-            send(CROSS, (CROSS, s, k), part, part, (me, (jx, jy)[k]))
+        if swap:
+            send((CROSS, s), (CROSS, s, k), part, part, (me, (jx, jy)[k]))
         send(PAIR, (PAIR, s), part, tokens.at[q, 1, :, columns(quarter)], (other, j))
 
     onwards = {}
@@ -510,9 +551,6 @@
             send((ONWARD, s, k - k % PLANE), (), part, part, device, line_recv.at[q, k], more)
 
     def cross_arrival(s, k):
-        if s in WHOLE:
-            line_arrival(s, k)
-            return
         q = sources[s]
         part = tokens.at[q, 0, :, columns(quarters[k])]
         arrive((CROSS, s, k - PLANE), part)
@@ -521,7 +559,7 @@
 
     def expert_up(s):
         q = sources[s]
-        arrive((), route.at[q] if s else route.at[q, 1], route_recv.at[q])
+        arrive((ROUTE, s), route.at[q, 1])
         if s == 0:
             loaded(gate_load, up_load)
         for p in range(CORES):
@@ -538,7 +576,7 @@
         q = sources[s]
         p = (t + c) % CORES
         if t == 0:
-            arrive((), route.at[q], route_recv.at[q])
+            arrive((ROUTE, s), route.at[q, 1])
             arrive((PAIR, s), tokens.at[q, 1])
         picks, _ = choice(s, p)
         taken = dot(picks.astype(bf16), tokens[q, p]).astype(bf16)
@@ -662,7 +700,7 @@
         gather_y((SHARED,), shared_hidden)
 
     def mixer_start():
-        arrive(EDGE, border)
+        pl.when(me > 0)(lambda: arrive(EDGE, border))
         loaded(outer_load, taps_load)
         extended[pad - edge_rows : pad, :] = border[...].astype(f32)
         places = (me * rows + lax.broadcasted_iota(jnp.int32, (rows, 1), 0)) % seq_length
@@ -694,7 +732,6 @@
     def mixer_end():
         loaded(gain_m_load, bias_m_load, gain_e_load, bias_e_load)
         stats_finish(0, mixed_ref[...], gain_m_ref, bias_m_ref, out_m_ref)
-        stores[0].start()
 
     def shared_dot():
         gather_finish((SHARED,), shared_hidden)
@@ -736,16 +773,22 @@
         mixer_end()
     with jax.named_scope("drain"):
         lines = tokens.at[0, 0, :, pl.ds(0, PLANE * cols)]
-        sent(UP, lines, z + 1 < chips)
-        sent(DOWN, lines, z > 0)
+        sent((UP, 0), lines, higher)
+        sent((DOWN, 0), lines, lower)
+        sent((UP, PLANE), lines, rising)
+        sent((DOWN, PLANE), lines, falling)
         for s, k in onwards:
             if k % PLANE == 0:
                 sent((ONWARD, s, k), lines, onwards[s, k][1])
-        sent(NEAR, route.at[0, 0])
+            if k == 0:
+                sent((ROUTE, s), route.at[0, 0], onwards[s, k][1])
+        sent(ROUTE_UP, route.at[0, 0], higher)
+        sent(ROUTE_DOWN, route.at[0, 0], lower)
         sent(PAIR, tokens.at[:, 0])
-        sent(ROUTE, route.at[pl.ds(0, chips - 1)])
-        sent(EDGE, edge)
-        sent(CROSS, tokens.at[pl.ds(0, chips - 1 - len(WHOLE)), 0, :, pl.ds(0, PLANE * cols)])
+        sent(ROUTE, route.at[:, 0])
+        sent(EDGE, edge, ~last)
+        sent((CROSS, 1), lines)
+        sent((CROSS, 2), lines, ~inner)
         gathered = pl.ds(0, (tp_count - 1) * cols)
         sent(HIDDEN, hidden.at[:, :, gathered])
         sent(SHARED, shared_hidden.at[:, gathered])
@@ -755,11 +798,8 @@
         sent((STATS, 0), stats_in.at[0])
     with jax.named_scope("finish"):
         stats_finish(1, total_ref[...], gain_e_ref, bias_e_ref, out_e_ref)
-    stores[1].start()
     with jax.named_scope("sent"):
         sent((STATS, 1), stats_in.at[1])
-        for store in stores:
-            store.wait()
 
 
 def pass_kernel(first_ref, second_ref, out_first_ref, out_second_ref):
@@ -797,10 +837,10 @@
     bf16, f32 = jnp.bfloat16, jnp.float32
     vmem = pl.BlockSpec(memory_space=pltpu.VMEM)
     hbm = pl.BlockSpec(memory_space=pl.ANY)
-    copies = 4 * chips + 20
+    copies = 5 * chips + 20
     weight = pltpu.VMEM((width, cols), bf16)
     scratch = [
-        *([pltpu.VMEM((rows, cols), bf16)] * 5),
+        *([pltpu.VMEM((rows, cols), bf16)] * 3),
         pltpu.VMEM(conv_taps.shape, bf16),
         pltpu.VMEM(route_ids.shape[::-1], jnp.int32),
         pltpu.VMEM(route_weights.shape[::-1], f32),
@@ -824,24 +864,15 @@
         pltpu.VMEM((rows, cols), f32),
         pltpu.VMEM((rows, cols), f32),
         pltpu.SemaphoreType.DMA((18,)),
-        pltpu.SemaphoreType.DMA((2,)),
-        pltpu.SemaphoreType.DMA((chips + 15,)),
+        pltpu.SemaphoreType.DMA((chips + 22,)),
         pltpu.SemaphoreType.DMA((copies,)),
         pltpu.SemaphoreType.DMA((chips, tp_count)),
         pltpu.SemaphoreType.DMA((chips,)),
         pltpu.SemaphoreType.DMA((chips,)),
     ]
     out = jax.ShapeDtypeStruct((rows, cols), bf16)
-    first, second = pl.pallas_call(
-        functools.partial(fused_kernel, (ep_count, tp_count, capacity, seq_length)),
-        out_shape=(out, out),
-        in_specs=[hbm] * 18,
-        out_specs=(hbm, hbm),
-        scratch_shapes=scratch,
-        compiler_params=pltpu.CompilerParams(
-            collective_id=0, has_side_effects=True, vmem_limit_bytes=VMEM_BYTES
-        ),
-    )(
+    near = pltpu.VMEM((rows, cols), bf16)
+    given = (
         outer_gate,
         inner_gate,
         conv_value,
@@ -861,8 +892,23 @@
         gain_experts,
         bias_experts,
     )
+    first, second = pl.pallas_call(
+        functools.partial(fused_kernel, (ep_count, tp_count, capacity, seq_length)),
+        out_shape=(near, near),
+        in_specs=[hbm] * 18,
+        out_specs=(vmem, vmem),
+        scratch_shapes=scratch,
+        compiler_params=pltpu.CompilerParams(
+            collective_id=0, has_side_effects=True, vmem_limit_bytes=VMEM_BYTES
+        ),
+    )(*(pltpu.with_memory_space_constraint(one, pltpu.HBM) for one in given))
     return pl.pallas_call(
-        pass_kernel, out_shape=(out, out), in_specs=[vmem, vmem], out_specs=(vmem, vmem)
+        pass_kernel,
+        out_shape=(out, out),
+        in_specs=[vmem, vmem],
+        out_specs=(vmem, vmem),
+        compiler_params=pltpu.CompilerParams(vmem_limit_bytes=SMALL_BYTES),
+
     )(first, second)
 
 

time: 60.7 us -> 58.9 us (0.970)
  Pallas kernels: 59.9 us -> 58.2 us
    pallas_call x1, Pallas kernels: 1.68 us -> 0.72 us  [fused_device(): pl.pallas_call(pass_kernel, out_shape=(out, out), in_specs=[vmem, vmem],...]
    pallas_call x1, Pallas kernels: 58.2 us -> 57.4 us  [fused_device(): pl.pallas_call(functools.partial(fused_kernel, (ep_count, tp_count, capac...]
where the time goes in v2:
time: 58.9 us; the launch traced here: 58.8 us
  Pallas kernels  58.2 us (99%)
  between operations  0.65 us (1%)
    pallas_call x1, Pallas kernels, fused_device(): pl.pallas_call(functools.partial(fused_kernel, (ep_count, tp_count, capac...  57.4 us

profile of v2, /device:TPU:0, one launch (start us, length us, event | category | flops | bytes accessed | tf_op | source)
XLA Modules:
  0.0 58.8 jit_solution(14675690360354056544)
XLA Ops:
  0.6 57.4 %shard_map.185 = (bf16[128,512]{1,0:T(8,128)(2,1)S(1)}, bf16[128,512]{1,0:T(8,128)(2,1)S(1)}) custom-call(bf16[128,512]{1,0:T(8,128)(2,1)} %outer_hbm.1, bf16[128,512]{1,0:T(8,128)(2,1)} %inner_hbm.1, bf16[128,512]{1,0:T(8,128)(2,1)} %value_hbm.1, bf16[3,512]{1,0:T(4,128)(2,1)} %taps_hbm.1, bf16[2048,512]{1,0:T(8,128)(2,1)} %mix_hbm.1, ...), custom_call_target="tpu_custom_call" | custom-call | tf_op jit(solution)/shard_map/pallas_call | solution.py:895
  58.1 0.7 %shard_map.186 = (bf16[128,512]{1,0:T(8,128)(2,1)}, bf16[128,512]{1,0:T(8,128)(2,1)}) custom-call(bf16[128,512]{1,0:T(8,128)(2,1)S(1)} %get-tuple-element.4.first_ref, bf16[128,512]{1,0:T(8,128)(2,1)S(1)} %get-tuple-element.5.second_ref), custom_call_target="tpu_custom_call" | custom-call | tf_op jit(solution)/shard_map/pallas_call | solution.py:905

commit v3 on v2

--- a/solution.py
+++ b/solution.py
@@ -168,11 +168,13 @@
         (ALL, act.shared, ()),
         (ALL, act.up, (0,)),
         (ALL, act.start_y, (0,)),
+        (ALL, act.start_x, (0, 0)),
         (ALL, act.line, (1, 0, True)),
         (INNER, act.line, (2, 0)),
-        (ALL, act.start_x, (0,)),
+        (ALL, act.start_x, (0, 1)),
         (ALL, act.line, (1, 1, True)),
         (INNER, act.line, (2, 1)),
+        (ALL, act.shared_relay, ()),
         (OUTER, act.line, (2, 0, True)),
         (INNER, act.line, (2, 2)),
         (INNER, act.line, (3, 0)),
@@ -181,7 +183,6 @@
         (INNER, act.line, (2, 3)),
         (OUTER, act.line, (2, 1, True)),
         (INNER, act.line, (3, 1)),
-        (ALL, act.shared_relay, ()),
         (ALL, act.up, (1,)),
         (ALL, act.start, (1,)),
         (INNER, act.line, (3, 2)),
@@ -197,30 +198,31 @@
         (OUTER, act.line, (3, 2)),
         (OUTER, act.line, (3, 3)),
         (INNER, act.relay, (1,)),
-        (INNER, act.relay, (2,)),
         (ALL, act.up_part, (3, 0)),
         (ALL, act.start_part, (3, 0)),
-        (OUTER, act.relay, (2,)),
+        (INNER, act.relay, (2,)),
         (ALL, act.up_part, (3, 1)),
         (ALL, act.start_part, (3, 1)),
         (INNER, act.down, (1,)),
         (INNER, act.give_back, (1,)),
+        (ALL, act.relay_part, (3, 0)),
         (INNER, act.down, (2,)),
-        (ALL, act.relay_part, (3, 0)),
+        (ALL, act.relay_part, (3, 1)),
         (INNER, act.give_back, (2,)),
-        (OUTER, act.down, (2,)),
-        (ALL, act.relay_part, (3, 1)),
+        (OUTER, act.relay, (2,)),
         (OUTER, act.relay, (1,)),
-        (OUTER, act.give_back, (2,)),
         (ALL, act.mixer, ()),
         (INNER, act.relay, (0,)),
         (ALL, act.down_part, (3, 0)),
         (ALL, act.give_back_part, (3, 0)),
         (ALL, act.down_part, (3, 1)),
         (ALL, act.give_back_part, (3, 1)),
+        (OUTER, act.down, (2,)),
+        (OUTER, act.give_back, (2,)),
         (OUTER, act.down, (1,)),
+        (ALL, act.mixer_relay, (0,)),
         (OUTER, act.give_back, (1,)),
-        (ALL, act.mixer_relay, ()),
+        (ALL, act.mixer_relay, (1,)),
         (ALL, act.down, (0,)),
         (ALL, act.give_back, (0,)),
         (ALL, act.mixer_dot, ()),
@@ -611,8 +613,9 @@
         def _():
             expert_return(s)
 
-    def start_x(s):
-        gather_x((HIDDEN, s), hidden.at[sources[s]])
+    def start_x(s, t=None):
+        ref = hidden.at[sources[s]] if t is None else part_ref(s, t)
+        gather_x((HIDDEN, s), ref)
 
     def start_y(s):
         gather_y((HIDDEN, s), hidden.at[sources[s]])
@@ -699,6 +702,9 @@
         gather_x((SHARED,), shared_hidden)
         gather_y((SHARED,), shared_hidden)
 
+    def mixer_ref(t):
+        return weighted.at[pl.ds(t * (rows // 2), rows // 2)]
+
     def mixer_start():
         pl.when(me > 0)(lambda: arrive(EDGE, border))
         loaded(outer_load, taps_load)
@@ -712,19 +718,21 @@
             kept = (places >= delay).astype(f32)
             convolved = convolved + taps_ref[offset : offset + 1, :].astype(f32) * delayed * kept
         weighted[:, columns(j)] = (outer_ref[...].astype(f32) * convolved).astype(bf16)
-        gather_x((MIXER,), weighted)
-        gather_y((MIXER,), weighted)
+        for t in range(2):
+            gather_x((MIXER, t), mixer_ref(t))
+            gather_y((MIXER, t), mixer_ref(t))
 
     def shared_relay():
         relay_x((SHARED,), shared_hidden)
         relay_y((SHARED,), shared_hidden)
 
-    def mixer_relay():
-        relay_x((MIXER,), weighted)
-        relay_y((MIXER,), weighted)
+    def mixer_relay(t):
+        relay_x((MIXER, t), mixer_ref(t))
+        relay_y((MIXER, t), mixer_ref(t))
 
     def mixer_dot():
-        gather_finish((MIXER,), weighted)
+        gather_finish((MIXER, 0), mixer_ref(0))
+        gather_finish((MIXER, 1), mixer_ref(1))
         loaded(mix_load)
         mixed_ref[...] = dot(weighted[...], mix_v[...])
         stats_start(0, mixed_ref[...])
@@ -837,7 +845,7 @@
     bf16, f32 = jnp.bfloat16, jnp.float32
     vmem = pl.BlockSpec(memory_space=pltpu.VMEM)
     hbm = pl.BlockSpec(memory_space=pl.ANY)
-    copies = 5 * chips + 20
+    copies = 5 * chips + 23
     weight = pltpu.VMEM((width, cols), bf16)
     scratch = [
         *([pltpu.VMEM((rows, cols), bf16)] * 3),

time: 58.9 us -> 58.4 us (level)
  Pallas kernels: 58.2 us -> 57.6 us
    pallas_call x1, Pallas kernels: 57.4 us -> 56.8 us  [fused_device(): pl.pallas_call(functools.partial(fused_kernel, (ep_count, tp_count, capac...]
where the time goes in v3:
time: 58.4 us; the launch traced here: 58.2 us
  Pallas kernels  57.6 us (99%)
  between operations  0.65 us (1%)
    pallas_call x1, Pallas kernels, fused_device(): pl.pallas_call(functools.partial(fused_kernel, (ep_count, tp_count, capac...  56.8 us

profile of v3, /device:TPU:0, one launch (start us, length us, event | category | flops | bytes accessed | tf_op | source)
XLA Modules:
  0.0 58.2 jit_solution(15691344203789280093)
XLA Ops:
  0.6 56.8 %shard_map.185 = (bf16[128,512]{1,0:T(8,128)(2,1)S(1)}, bf16[128,512]{1,0:T(8,128)(2,1)S(1)}) custom-call(bf16[128,512]{1,0:T(8,128)(2,1)} %outer_hbm.1, bf16[128,512]{1,0:T(8,128)(2,1)} %inner_hbm.1, bf16[128,512]{1,0:T(8,128)(2,1)} %value_hbm.1, bf16[3,512]{1,0:T(4,128)(2,1)} %taps_hbm.1, bf16[2048,512]{1,0:T(8,128)(2,1)} %mix_hbm.1, ...), custom_call_target="tpu_custom_call" | custom-call | tf_op jit(solution)/shard_map/pallas_call | solution.py:903
  57.5 0.7 %shard_map.186 = (bf16[128,512]{1,0:T(8,128)(2,1)}, bf16[128,512]{1,0:T(8,128)(2,1)}) custom-call(bf16[128,512]{1,0:T(8,128)(2,1)S(1)} %get-tuple-element.4.first_ref, bf16[128,512]{1,0:T(8,128)(2,1)S(1)} %get-tuple-element.5.second_ref), custom_call_target="tpu_custom_call" | custom-call | tf_op jit(solution)/shard_map/pallas_call | solution.py:913

commit v4 on v3

--- a/solution.py
+++ b/solution.py
@@ -218,8 +218,8 @@
         (ALL, act.down_part, (3, 1)),
         (ALL, act.give_back_part, (3, 1)),
         (OUTER, act.down, (2,)),
+        (OUTER, act.down, (1,)),
         (OUTER, act.give_back, (2,)),
-        (OUTER, act.down, (1,)),
         (ALL, act.mixer_relay, (0,)),
         (OUTER, act.give_back, (1,)),
         (ALL, act.mixer_relay, (1,)),

time: 58.4 us -> 57.8 us (0.990)
  Pallas kernels: 57.6 us -> 56.9 us
    pallas_call x1, Pallas kernels: 56.8 us -> 56.2 us  [fused_device(): pl.pallas_call(functools.partial(fused_kernel, (ep_count, tp_count, capac...]
where the time goes in v4:
time: 57.8 us; the launch traced here: 57.5 us
  Pallas kernels  56.9 us (98%)
  between operations  0.65 us (1%)
    pallas_call x1, Pallas kernels, fused_device(): pl.pallas_call(functools.partial(fused_kernel, (ep_count, tp_count, capac...  56.2 us

profile of v4, /device:TPU:0, one launch (start us, length us, event | category | flops | bytes accessed | tf_op | source)
XLA Modules:
  0.0 57.5 jit_solution(8078784941131184755)
XLA Ops:
  0.6 56.2 %shard_map.185 = (bf16[128,512]{1,0:T(8,128)(2,1)S(1)}, bf16[128,512]{1,0:T(8,128)(2,1)S(1)}) custom-call(bf16[128,512]{1,0:T(8,128)(2,1)} %outer_hbm.1, bf16[128,512]{1,0:T(8,128)(2,1)} %inner_hbm.1, bf16[128,512]{1,0:T(8,128)(2,1)} %value_hbm.1, bf16[3,512]{1,0:T(4,128)(2,1)} %taps_hbm.1, bf16[2048,512]{1,0:T(8,128)(2,1)} %mix_hbm.1, ...), custom_call_target="tpu_custom_call" | custom-call | tf_op jit(solution)/shard_map/pallas_call | solution.py:903
  56.8 0.7 %shard_map.186 = (bf16[128,512]{1,0:T(8,128)(2,1)}, bf16[128,512]{1,0:T(8,128)(2,1)}) custom-call(bf16[128,512]{1,0:T(8,128)(2,1)S(1)} %get-tuple-element.4.first_ref, bf16[128,512]{1,0:T(8,128)(2,1)S(1)} %get-tuple-element.5.second_ref), custom_call_target="tpu_custom_call" | custom-call | tf_op jit(solution)/shard_map/pallas_call | solution.py:913

commit v5 on v4

--- a/solution.py
+++ b/solution.py
@@ -564,8 +564,8 @@
         arrive((ROUTE, s), route.at[q, 1])
         if s == 0:
             loaded(gate_load, up_load)
-        for p in range(CORES):
-            picks, _ = choice(s, p)
+        chosen = [choice(s, p)[0] for p in range(CORES)]
+        for p, picks in enumerate(chosen):
             if p == 1:
                 arrive((PAIR, s), tokens.at[q, 1])
             rows_in[p * capacity : (p + 1) * capacity, :] = dot(
@@ -579,8 +579,9 @@
         p = (t + c) % CORES
         if t == 0:
             arrive((ROUTE, s), route.at[q, 1])
+        picks, _ = choice(s, p)
+        if t == 0:
             arrive((PAIR, s), tokens.at[q, 1])
-        picks, _ = choice(s, p)
         taken = dot(picks.astype(bf16), tokens[q, p]).astype(bf16)
         held = silu(dot(taken, gate_v[...])) * dot(taken, up_v[...])
         hidden[q, t * capacity : (t + 1) * capacity, columns(j)] = held.astype(bf16)
@@ -590,8 +591,8 @@
 
     def down_part(s, t):
         q = sources[s]
+        picks, weight = choice(s, (t + c) % CORES)
         gather_finish((HIDDEN, s, t), part_ref(s, t))
-        picks, weight = choice(s, (t + c) % CORES)
         full = dot(hidden[q, t * capacity : (t + 1) * capacity], down_v[...])
         scale = jnp.sum(picks * weight, axis=1, keepdims=True)
         scaled = (full * scale).astype(bf16)

time: 57.8 us -> 57.8 us (level)
  no operation moved by 1% of the time
where the time goes in v5:
time: 57.8 us; the launch traced here: 57.5 us
  Pallas kernels  56.9 us (98%)
  between operations  0.65 us (1%)
    pallas_call x1, Pallas kernels, fused_device(): pl.pallas_call(functools.partial(fused_kernel, (ep_count, tp_count, capac...  56.2 us

profile of v5, /device:TPU:0, one launch (start us, length us, event | category | flops | bytes accessed | tf_op | source)
XLA Modules:
  0.0 57.5 jit_solution(4067189043960663232)
XLA Ops:
  0.6 56.2 %shard_map.185 = (bf16[128,512]{1,0:T(8,128)(2,1)S(1)}, bf16[128,512]{1,0:T(8,128)(2,1)S(1)}) custom-call(bf16[128,512]{1,0:T(8,128)(2,1)} %outer_hbm.1, bf16[128,512]{1,0:T(8,128)(2,1)} %inner_hbm.1, bf16[128,512]{1,0:T(8,128)(2,1)} %value_hbm.1, bf16[3,512]{1,0:T(4,128)(2,1)} %taps_hbm.1, bf16[2048,512]{1,0:T(8,128)(2,1)} %mix_hbm.1, ...), custom_call_target="tpu_custom_call" | custom-call | tf_op jit(solution)/shard_map/pallas_call | solution.py:904
  56.8 0.7 %shard_map.186 = (bf16[128,512]{1,0:T(8,128)(2,1)}, bf16[128,512]{1,0:T(8,128)(2,1)}) custom-call(bf16[128,512]{1,0:T(8,128)(2,1)S(1)} %get-tuple-element.4.first_ref, bf16[128,512]{1,0:T(8,128)(2,1)S(1)} %get-tuple-element.5.second_ref), custom_call_target="tpu_custom_call" | custom-call | tf_op jit(solution)/shard_map/pallas_call | solution.py:914
